TPU v7x, 32 devices: a whole 2x2x4 slice. The times are simulated.
32 devices in a mesh: sp: 8 (over z, y), tp: 4 (over x, core).
Axes of the slice: x: 2, y: 2, z: 4, core: 2. Of those that a mesh axis runs over, the one named last changes fastest.
Arguments:
- middle_stream: bfloat16 [1536, 2048], P('sp', 'tp'), may hold values from -6 to 6
- output_gradient: bfloat16 [1536, 2048], P('sp', 'tp'), may hold values from -6 to 6
- routes: int32 [1536, 2], P('sp'), may hold values from 0 to 7, all different within a row; in each aligned block of 192 rows (0 to 191, 192 to 383, ...) at most 72 rows name the same one
- chosen_expert_weight: float32 [1536, 2], P('sp'), may hold values from 0.2 to 1
- expert_gate_weight: bfloat16 [8, 2048, 3584], P('sp', None, 'tp'), may hold values from -0.125 to 0.125
- expert_up_weight: bfloat16 [8, 2048, 3584], P('sp', None, 'tp'), may hold values from -0.125 to 0.125
- expert_down_weight: bfloat16 [8, 3584, 2048], P('sp', 'tp'), may hold values from -0.09375 to 0.09375
- recurrent_output_weight: bfloat16 [2048, 1024], P(None, 'tp'), may hold values from -0.1875 to 0.1875
- recurrence_input: bfloat16 [1536, 1024], P('sp', 'tp'), may hold values from -8 to 8
- output_gate_logits: bfloat16 [1536, 1024], P('sp', 'tp'), may hold values from -6 to 6
- recurrence_gate_weight: bfloat16 [8, 128, 128], replicated, may hold values from -0.5 to 0.5
- input_gate_weight: bfloat16 [8, 128, 128], replicated, may hold values from -0.5 to 0.5
- channel_decay_param: float32 [1024], P('tp'), may hold values from 4 to 13
- extra_log_decay: float32 [1536, 1024], P('sp', 'tp'), may hold values from -0.7 to 0
Outputs:
- grad_gate: bfloat16 [8, 2048, 3584], P('sp', None, 'tp')
- grad_up: bfloat16 [8, 2048, 3584], P('sp', None, 'tp')
- grad_down: bfloat16 [8, 3584, 2048], P('sp', 'tp')
- grad_out_proj: float32 [2048, 1024], P('sp', 'tp')
- grad_input: float32 [1536, 1024], P('sp', 'tp')
- grad_gate_pre: float32 [1536, 1024], P('sp', 'tp')
Inputs may be any that keep to these rules, and one draw needn't show every extreme that they name: `routes`: in the rows of one index of sp no expert is named more than 72 times, a bound that some block reaches in some of them; the entries of a row differ.
All inputs are finite; a program needn't handle non-finite values.
Results may differ from a plain program's by a relative error of at most 0.017.
Values may be sent and summed in bfloat16 or wider, within the bound.
A program may use at most 128 MiB of HBM per device.

v0:
```python
import functools

import jax
import jax.numpy as jnp
from jax import lax
from jax.experimental import pallas as pl
from jax.experimental.pallas import tpu as pltpu
from jax.sharding import PartitionSpec as P

MESH = pl.DeviceIdType.MESH


def partner(t, stage, m):
    d = m >> (stage + 1)
    return t + d * (1 - 2 * ((t // d) % 2))


def held_columns(t, stage, m):
    if stage == 0:
        return [t]
    return held_columns(t, stage - 1, m) + held_columns(partner(t, stage - 1, m), stage - 1, m)


def greet(peers):
    barrier = pltpu.get_barrier_semaphore()
    for peer in peers:
        pl.semaphore_signal(barrier, inc=1, device_id=peer, device_id_type=MESH)
    pl.semaphore_wait(barrier, len(peers))


def remote(src, dst, send_sem, recv_sem, peer):
    return pltpu.make_async_remote_copy(
        src_ref=src,
        dst_ref=dst,
        send_sem=send_sem,
        recv_sem=recv_sem,
        device_id=peer,
        device_id_type=MESH,
    )


def shifted(value, k, fill, reverse):
    pad = jnp.full((k, value.shape[1]), fill, value.dtype)
    if reverse:
        return jnp.concatenate([value[k:], pad], axis=0)
    return jnp.concatenate([pad, value[:-k]], axis=0)


def local_scan(gain, term, reverse):
    k = 1
    while k < gain.shape[0]:
        term = term + gain * shifted(term, k, 0.0, reverse)
        gain = gain * shifted(gain, k, 1.0, reverse)
        k *= 2
    return gain, term


def dispatch_kernel(
    n,
    m,
    send_ref,
    decay_ref,
    driven_ref,
    out_ref,
    states_ref,
    prev_ref,
    gain_buf,
    car_send,
    car_buf,
    a2a_send,
    a2a_recv,
    tp_send,
    tp_recv,
    car_ssem,
    car_rsem,
    self_sem,
):
    s, t = lax.axis_index("sp"), lax.axis_index("tp")
    feat = send_ref.shape[3]
    stages = m.bit_length() - 1
    greet(
        [{"sp": lax.rem(s + k, n)} for k in range(1, n)]
        + [{"tp": partner(t, j, m)} for j in range(stages)]
    )

    def block(src, col):
        return out_ref.at[:, src, :, pl.ds(pl.multiple_of(col * feat, feat), feat)]

    first = []
    own = pltpu.make_async_copy(send_ref.at[:, s], block(s, t), self_sem)
    own.start()
    for k in range(1, n):
        dst = lax.rem(s + k, n)
        copy = remote(
            send_ref.at[:, dst], block(s, t), a2a_send.at[k], a2a_recv.at[k], {"sp": dst}
        )
        copy.start()
        first.append(copy)

    pushed = []

    def push(k, stage, i, col):
        src = lax.rem(s + n - k, n)
        at = 2**stage - 1 + i
        copy = remote(
            block(src, col),
            block(src, col),
            tp_send.at[at, k],
            tp_recv.at[at, k],
            {"tp": partner(t, stage, m)},
        )
        copy.start()
        pushed.append(copy)

    def arrived(k, stage):
        src = lax.rem(s + n - k, n)
        cols = held_columns(partner(t, stage, m), stage, m)
        for i, col in enumerate(cols):
            at = 2**stage - 1 + i
            remote(
                block(src, col),
                block(src, col),
                tp_send.at[at, k],
                tp_recv.at[at, k],
                {"tp": partner(t, stage, m)},
            ).wait_recv()
            for later in range(stage + 1, stages):
                push(k, later, 2**stage + i, col)

    def forward(k):
        if k == 0:
            own.wait()
        else:
            first[k - 1].wait_recv()
        for stage in range(stages):
            push(k, stage, 0, t)

    forward(0)
    gain, term = local_scan(decay_ref[...], driven_ref[...], False)
    gain_buf[...] = gain
    states_ref[...] = term
    rows = gain.shape[0]
    car_send[0:1] = gain[rows - 1 : rows]
    car_send[1:2] = term[rows - 1 : rows]
    forward(1)
    carries = []
    for k in range(1, n):
        copy = remote(
            car_send, car_buf.at[k], car_ssem.at[k], car_rsem.at[k], {"sp": lax.rem(s + k, n)}
        )
        copy.start()
        carries.append(copy)
    for k in range(2, n):
        forward(k)
        for stage in range(stages - 1):
            arrived(k - 2, stage)
    for copy in carries:
        copy.wait()
    carry = jnp.zeros((1, gain_buf.shape[1]), jnp.float32)
    for k in range(n - 1, 0, -1):
        carry = jnp.where(k <= s, car_buf[k, 0:1] * carry + car_buf[k, 1:2], carry)
    states = states_ref[...] + gain_buf[...] * carry
    states_ref[...] = states
    prev_ref[...] = jnp.concatenate([carry, states[:-1]], axis=0)
    for k in range(n - 2, n):
        for stage in range(stages - 1):
            arrived(k, stage)
    for k in range(n):
        arrived(k, stages - 1)
    for copy in first:
        copy.wait_send()
    for copy in pushed:
        copy.wait_send()


def dispatch(send, decay, driven):
    n, m = lax.axis_size("sp"), lax.axis_size("tp")
    two, _, cap, feat = send.shape
    rows, channels = decay.shape
    vmem = pl.BlockSpec(memory_space=pltpu.VMEM)
    state = jax.ShapeDtypeStruct((rows, channels), jnp.float32)
    return pl.pallas_call(
        functools.partial(dispatch_kernel, n, m),
        out_shape=(jax.ShapeDtypeStruct((two, n, cap, m * feat), send.dtype), state, state),
        in_specs=[vmem] * 3,
        out_specs=(vmem,) * 3,
        scratch_shapes=[
            pltpu.VMEM((rows, channels), jnp.float32),
            pltpu.VMEM((2, channels), jnp.float32),
            pltpu.VMEM((n, 2, channels), jnp.float32),
            pltpu.SemaphoreType.DMA((n,)),
            pltpu.SemaphoreType.DMA((n,)),
            pltpu.SemaphoreType.DMA((m - 1, n)),
            pltpu.SemaphoreType.DMA((m - 1, n)),
            pltpu.SemaphoreType.DMA((n,)),
            pltpu.SemaphoreType.DMA((n,)),
            pltpu.SemaphoreType.DMA,
        ],
        compiler_params=pltpu.CompilerParams(collective_id=0, has_side_effects=True),
        name="dispatch",
    )(send, decay, driven)


def tail_kernel(
    n,
    decay_ref,
    input_ref,
    part_ref,
    grad_ref,
    sum_ref,
    gain_buf,
    car_send,
    car_buf,
    part_buf,
    part_ssem,
    part_rsem,
    car_ssem,
    car_rsem,
):
    s = lax.axis_index("sp")
    greet([{"sp": lax.rem(s + k, n)} for k in range(1, n)])
    parts = []
    for k in range(1, n):
        dst = lax.rem(s + k, n)
        copy = remote(
            part_ref.at[dst], part_buf.at[k], part_ssem.at[k], part_rsem.at[k], {"sp": dst}
        )
        parts.append(copy)
    decay = decay_ref[...]
    gain, term = local_scan(shifted(decay, 1, 1.0, True), input_ref[...], True)
    gain_buf[...] = gain
    grad_ref[...] = term
    car_send[0:1] = decay[0:1] * gain[0:1]
    car_send[1:2] = decay[0:1] * term[0:1]
    carries = []
    for k in range(1, n):
        copy = remote(
            car_send, car_buf.at[k], car_ssem.at[k], car_rsem.at[k], {"sp": lax.rem(s + k, n)}
        )
        copy.start()
        carries.append(copy)
    for copy in parts:
        copy.start()
    for copy in carries:
        copy.wait()
    carry = jnp.zeros((1, gain_buf.shape[1]), jnp.float32)
    for k in range(1, n):
        carry = jnp.where(k > s, car_buf[k, 0:1] * carry + car_buf[k, 1:2], carry)
    grad_ref[...] = grad_ref[...] + gain_buf[...] * carry
    sum_ref[...] = part_ref[s].astype(jnp.float32)
    for k in range(1, n):
        parts[k - 1].wait()
        sum_ref[...] += part_buf[k].astype(jnp.float32)


def tail(decay, state_in, part):
    n = lax.axis_size("sp")
    rows, channels = decay.shape
    vmem = pl.BlockSpec(memory_space=pltpu.VMEM)
    return pl.pallas_call(
        functools.partial(tail_kernel, n),
        out_shape=(
            jax.ShapeDtypeStruct((rows, channels), jnp.float32),
            jax.ShapeDtypeStruct(part.shape[1:], jnp.float32),
        ),
        in_specs=[vmem] * 3,
        out_specs=(vmem,) * 2,
        scratch_shapes=[
            pltpu.VMEM((rows, channels), jnp.float32),
            pltpu.VMEM((2, channels), jnp.float32),
            pltpu.VMEM((n, 2, channels), jnp.float32),
            pltpu.VMEM(part.shape, part.dtype),
            pltpu.SemaphoreType.DMA((n,)),
            pltpu.SemaphoreType.DMA((n,)),
            pltpu.SemaphoreType.DMA((n,)),
            pltpu.SemaphoreType.DMA((n,)),
        ],
        compiler_params=pltpu.CompilerParams(collective_id=1, has_side_effects=True),
        name="tail",
    )(decay, state_in, part)


def gelu_parts(output_gate_logits):
    gate_float = output_gate_logits.astype(jnp.float32)
    return jax.jvp(jax.nn.gelu, (gate_float,), (jnp.ones_like(gate_float),))


def expert_backward(inputs, cotangent, gate_weight, up_weight, down_weight):
    gate_act = jnp.dot(inputs, gate_weight, preferred_element_type=jnp.float32)
    up_act = jnp.dot(inputs, up_weight, preferred_element_type=jnp.float32)
    sigmoid_gate = jax.nn.sigmoid(gate_act)
    silu_act = gate_act * sigmoid_gate
    hidden = (silu_act * up_act).astype(jnp.bfloat16)
    d_hidden = lax.dot_general(
        cotangent, down_weight, (((1,), (1,)), ((), ())), preferred_element_type=jnp.float32
    )
    grad_down = lax.dot_general(
        hidden, cotangent, (((0,), (0,)), ((), ())), preferred_element_type=jnp.float32
    )
    d_gate = (d_hidden * up_act * sigmoid_gate * (1.0 + gate_act * (1.0 - sigmoid_gate))).astype(
        jnp.bfloat16
    )
    d_up = (d_hidden * silu_act).astype(jnp.bfloat16)
    grad_gate = lax.dot_general(
        inputs, d_gate, (((0,), (0,)), ((), ())), preferred_element_type=jnp.float32
    )
    grad_up = lax.dot_general(
        inputs, d_up, (((0,), (0,)), ((), ())), preferred_element_type=jnp.float32
    )
    partial_value = lax.dot_general(
        d_gate, gate_weight, (((1,), (1,)), ((), ())), preferred_element_type=jnp.float32
    )
    partial_value = partial_value + lax.dot_general(
        d_up, up_weight, (((1,), (1,)), ((), ())), preferred_element_type=jnp.float32
    )
    return (
        grad_gate.astype(jnp.bfloat16),
        grad_up.astype(jnp.bfloat16),
        grad_down.astype(jnp.bfloat16),
        partial_value,
    )


def per_device(
    middle_stream,
    output_gradient,
    routes,
    chosen_expert_weight,
    expert_gate_weight,
    expert_up_weight,
    expert_down_weight,
    recurrent_output_weight,
    recurrence_input,
    output_gate_logits,
    recurrence_gate_weight,
    input_gate_weight,
    channel_decay_param,
    extra_log_decay,
):
    rows_dev = middle_stream.shape[0]
    top_count = routes.shape[1]
    experts = lax.axis_size("sp")
    capacity = 3 * top_count * rows_dev // (2 * experts)
    feat_width = middle_stream.shape[1]
    choice = routes.T
    expert_ids = jnp.arange(experts, dtype=jnp.int32)
    named = [(choice[k][None, :] == expert_ids[:, None]) for k in range(top_count)]
    named_any = sum(part.astype(jnp.bfloat16) for part in named)
    position = jnp.arange(rows_dev, dtype=jnp.int32)
    earlier = (position[:, None] < position[None, :]).astype(jnp.bfloat16)
    rank = jnp.dot(named_any, earlier, preferred_element_type=jnp.float32).astype(jnp.int32)
    slot_ids = jnp.arange(experts * capacity, dtype=jnp.int32)
    picks = []
    for k in range(top_count):
        slot = jnp.sum(
            jnp.where(named[k], rank + expert_ids[:, None] * capacity, 0), axis=0, keepdims=True
        )
        picks.append((slot_ids[:, None] == slot).astype(jnp.bfloat16))
    pick_any = sum(picks)
    pick_both = jnp.concatenate(picks, axis=1)
    pair_cot = (
        chosen_expert_weight.T[:, :, None] * output_gradient.astype(jnp.float32)[None]
    ).astype(jnp.bfloat16)
    pair_cot = pair_cot.reshape(-1, feat_width)
    send_rows = jnp.dot(pick_any, middle_stream, preferred_element_type=jnp.bfloat16)
    send_cot = jnp.dot(pick_both, pair_cot, preferred_element_type=jnp.bfloat16)
    send = jnp.stack([send_rows, send_cot]).reshape(2, experts, capacity, feat_width)
    channels = recurrence_input.shape[1]
    block_width = recurrence_gate_weight.shape[1]
    local_blocks = channels // block_width
    first_block = lax.axis_index("tp") * local_blocks
    recall_weight = lax.dynamic_slice_in_dim(recurrence_gate_weight, first_block, local_blocks, 0)
    admit_weight = lax.dynamic_slice_in_dim(input_gate_weight, first_block, local_blocks, 0)
    u_blocks = recurrence_input.reshape(rows_dev, local_blocks, block_width)
    forget_gate = jax.nn.sigmoid(
        jnp.einsum(
            "tnb,nbc->tnc", u_blocks, recall_weight, preferred_element_type=jnp.float32
        ).reshape(rows_dev, channels)
    )
    admit_gate = jax.nn.sigmoid(
        jnp.einsum(
            "tnb,nbc->tnc", u_blocks, admit_weight, preferred_element_type=jnp.float32
        ).reshape(rows_dev, channels)
    )
    baseline_rate = jax.nn.softplus(-channel_decay_param)
    decay_logarithm = -8.0 * forget_gate * baseline_rate[None, :] + extra_log_decay
    decay_step = jnp.exp(decay_logarithm)
    input_scale = jnp.sqrt(-jnp.expm1(2.0 * decay_logarithm))
    u_float = recurrence_input.astype(jnp.float32)
    driven = u_float * admit_gate * input_scale
    received, states, prev_states = dispatch(send, decay_step, driven)
    row_width = received.shape[3]
    inputs = received[0].reshape(-1, row_width)
    cotangent = received[1].reshape(-1, row_width)
    grad_gate, grad_up, grad_down, partial_value = expert_backward(
        inputs, cotangent, expert_gate_weight[0], expert_up_weight[0], expert_down_weight[0]
    )
    slot_grad = lax.psum_scatter(
        partial_value.astype(jnp.bfloat16), "tp", scatter_dimension=1, tiled=True
    )
    returned = lax.all_to_all(slot_grad[None], "sp", split_axis=1, concat_axis=0, tiled=True)
    arrived = lax.dot_general(
        pick_any,
        returned.reshape(experts * capacity, -1),
        (((0,), (0,)), ((), ())),
        preferred_element_type=jnp.float32,
    )
    residual_grad = (output_gradient.astype(jnp.float32) + arrived).astype(jnp.bfloat16)
    grad_full = lax.all_gather(residual_grad, "tp", axis=1, tiled=True)
    mixer_grad = jnp.dot(grad_full, recurrent_output_weight, preferred_element_type=jnp.float32)
    gelu_val, gelu_der = gelu_parts(output_gate_logits)
    lru_out = (states * gelu_val).astype(jnp.bfloat16)
    gop_part = lax.dot_general(
        grad_full, lru_out, (((0,), (0,)), ((), ())), preferred_element_type=jnp.float32
    ).astype(jnp.bfloat16)
    gop_part = gop_part.reshape(experts, -1, channels)
    grad_gate_pre = mixer_grad * states * gelu_der
    state_in = mixer_grad * gelu_val
    state_grad, grad_out_proj = tail(decay_step, state_in, gop_part)
    d_log = state_grad * (
        prev_states * decay_step - u_float * admit_gate * decay_step * decay_step / input_scale
    )
    d_recall = (d_log * (-8.0 * baseline_rate[None, :]) * forget_gate * (1.0 - forget_gate)).astype(
        jnp.bfloat16
    )
    d_admit = (state_grad * u_float * input_scale * admit_gate * (1.0 - admit_gate)).astype(
        jnp.bfloat16
    )
    back_recall = jnp.einsum(
        "tnc,nbc->tnb",
        d_recall.reshape(rows_dev, local_blocks, block_width),
        recall_weight,
        preferred_element_type=jnp.float32,
    )
    back_admit = jnp.einsum(
        "tnc,nbc->tnb",
        d_admit.reshape(rows_dev, local_blocks, block_width),
        admit_weight,
        preferred_element_type=jnp.float32,
    )
    grad_input = state_grad * admit_gate * input_scale + (back_recall + back_admit).reshape(
        rows_dev, channels
    )
    return (
        grad_gate[None],
        grad_up[None],
        grad_down[None],
        grad_out_proj,
        grad_input,
        grad_gate_pre,
    )


def solution(mesh):
    placed = (
        P("sp", "tp"),
        P("sp", "tp"),
        P("sp", None),
        P("sp", None),
        P("sp", None, "tp"),
        P("sp", None, "tp"),
        P("sp", "tp", None),
        P(None, "tp"),
        P("sp", "tp"),
        P("sp", "tp"),
        P(),
        P(),
        P("tp"),
        P("sp", "tp"),
    )
    return jax.shard_map(
        per_device,
        mesh=mesh,
        in_specs=placed,
        out_specs=(
            P("sp", None, "tp"),
            P("sp", None, "tp"),
            P("sp", "tp", None),
            P("sp", "tp"),
            P("sp", "tp"),
            P("sp", "tp"),
        ),
        check_vma=False,
    )
```

profile of v0, /device:TPU:12, one launch (start us, length us, event | category | flops | bytes accessed | tf_op | source)
XLA Modules:
  0.0 201.1 jit_solution(11796987618169147826)
XLA Ops:
  7.3 0.8 fusion.103
  8.1 1.0 convert_element_type.86
  9.2 0.9 broadcast_compare_fusion.1
  10.1 1.2 fusion.33
  11.4 1.1 fusion.18
  12.6 1.0 fusion.22
  13.7 0.8 fusion.63
  15.9 1.1 pad_maximum_fusion.send_ref
  17.0 42.8 %dispatch.1 = (bf16[2,8,72,2048]{3,2,1,0:T(8,128)(2,1)}, f32[192,256]{1,0:T(8,128)}, f32[192,256]{1,0:T(8,128)}) custom-call(bf16[2,8,72,512]{3,2,1,0:T(8,128)(2,1)} %pad_maximum_fusion.send_ref, f32[192,256]{1,0:T(8,128)} %exp.22.decay_ref, f32[192,256]{1,0:T(8,128)} %get-tuple-element.18.driven_ref), custom_call_target="tpu_custom_call" | custom-call | tf_op jit(solution)/shard_map/dispatch/pallas_call | solution.py:182
  59.8 2.9 %fusion.102 = (bf16[1,8,72,2048]{3,2,1,0:T(8,128)(2,1)S(1)}, bf16[1,8,72,2048]{3,2,1,0:T(8,128)(2,1)S(1)}) fusion(bf16[2,8,72,2048]{3,2,1,0:T(8,128)(2,1)} %get-tuple-element.11), kind=kLoop, calls=%fused_computation.139 | loop fusion | bytes 9437184 | tf_op jit(solution)/shard_map/slice | solution.py:394
  63.2 2.6 %fusion.2 = f32[576,896]{1,0:T(8,128)S(1)} fusion(bf16[576,2048]{1,0:T(8,128)(2,1)S(1)} %bitcast.130, bf16[1,2048,896]{2,1,0:T(8,128)(2,1)S(1)} %copy-done.12), kind=kOutput, calls=%fused_computation.3 | convolution fusion | flops 2113929216 | bytes 8093696 | tf_op jit(solution)/shard_map/dot_general | solution.py:289
  66.4 2.6 %fusion.6 = f32[576,896]{1,0:T(8,128)S(1)} fusion(bf16[576,2048]{1,0:T(8,128)(2,1)S(1)} %bitcast.131, bf16[1,2048,896]{2,1,0:T(8,128)(2,1)S(1)} %copy-done.13), kind=kOutput, calls=%fused_computation.7 | convolution fusion | flops 2113929216 | bytes 8093696 | tf_op jit(solution)/shard_map/dot_general | solution.py:290
  69.2 3.2 %multiply_convert_fusion.1 = (bf16[576,896]{1,0:T(8,128)(2,1)S(1)}, bf16[576,896]{1,0:T(8,128)(2,1)S(1)}) fusion(f32[576,896]{1,0:T(8,128)S(1)} %fusion.2, f32[576,896]{1,0:T(8,128)S(1)} %fusion.6, bf16[576,2048]{1,0:T(8,128)(2,1)S(1)} %bitcast.128, bf16[1,896,2048]{2,1,0:T(8,128)(2,1)S(1)} %copy-done.11), kind=kOutput, calls=%fused_computation.16 | convolution fusion | flops 2120638464 | bytes 12222464 | tf_op jit(solution)/shard_map/dot_general | solution.py:294
  72.4 2.7 %fusion = f32[576,2048]{1,0:T(8,128)S(1)} fusion(bf16[576,896]{1,0:T(8,128)(2,1)S(1)} %get-tuple-element.23, bf16[1,2048,896]{2,1,0:T(8,128)(2,1)S(1)} %copy-done.12), kind=kOutput, calls=%fused_computation.1 | convolution fusion | flops 2113929216 | bytes 9420800 | tf_op jit(solution)/shard_map/dot_general | solution.py:310
  75.1 3.9 %add_convert_fusion = bf16[576,2048]{1,0:T(8,128)(2,1)} fusion(f32[576,2048]{1,0:T(8,128)S(1)} %fusion, bf16[576,896]{1,0:T(8,128)(2,1)S(1)} %get-tuple-element.22, bf16[1,2048,896]{2,1,0:T(8,128)(2,1)S(1)} %copy-done.13), kind=kOutput, calls=%fused_computation | convolution fusion | flops 2116288512 | bytes 11780096 | tf_op jit(solution)/shard_map/dot_general | solution.py:313
  79.1 6.9 %convert_bitcast_fusion.1 = bf16[1,2048,896]{2,1,0:T(8,128)(2,1)} fusion(bf16[576,2048]{1,0:T(8,128)(2,1)} %bitcast.132, bf16[576,896]{1,0:T(8,128)(2,1)S(1)} %get-tuple-element.22), kind=kOutput, calls=%fused_computation.12 | convolution fusion | flops 2115764224 | bytes 7061504 | tf_op jit(solution)/shard_map/dot_general | solution.py:307
  85.9 31.8 %reduce-scatter.2.cloned.1.call-done = bf16[576,512]{1,0:T(8,128)(2,1)} async-done(((bf16[576,2048]{1,0:T(8,128)(2,1)}), bf16[576,512]{1,0:T(8,128)(2,1)}) %reduce-scatter.2.cloned.1.call-update) | async-done | bytes 589840 | tf_op jit(solution)/shard_map/reduce_scatter | solution.py:398
  117.7 2.0 copy.88
  120.2 4.2 %reduce = bf16[576,512]{1,0:T(8,128)(2,1)S(1)} reduce(bf16[576,1,512]{2,1,0:T(2,128)(2,1)S(1)} %bitcast.127, bf16[]{:T(256)} %broadcast.143), dimensions={1}, to_apply=%bitcast.126.reduce_sub_computation | reduce | bytes 1179650
  124.4 1.1 reshape.131
  125.5 6.1 %all-to-all-start = ((bf16[8,2,18432]{2,1,0:T(2,128)(2,1)}), bf16[8,2,18432]{2,1,0:T(2,128)(2,1)S(1)}, u32[]{:S(2)}, u32[]{:S(2)}) async-start(bf16[8,2,18432]{2,1,0:T(2,128)(2,1)} %reshape.131), calls=%async_computation.1 | async-start | bytes 1179648 | tf_op jit(solution)/shard_map/all_to_all | solution.py:401
  131.6 7.3 %convert_bitcast_fusion.2 = bf16[1,2048,896]{2,1,0:T(8,128)(2,1)} fusion(bf16[576,2048]{1,0:T(8,128)(2,1)} %bitcast.133, bf16[576,896]{1,0:T(8,128)(2,1)} %copy-done.16), kind=kOutput, calls=%fused_computation.13 | convolution fusion | flops 2115764224 | bytes 7061504 | tf_op jit(solution)/shard_map/dot_general | solution.py:304
  138.8 4.6 %convert_bitcast_fusion = bf16[1,896,2048]{2,1,0:T(8,128)(2,1)} fusion(bf16[576,2048]{1,0:T(8,128)(2,1)S(1)} %bitcast.129, f32[576,896]{1,0:T(8,128)S(1)} %copy-done.20, f32[576,896]{1,0:T(8,128)S(1)} %copy-done.18), kind=kOutput, calls=%fused_computation.11 | convolution fusion | flops 2118860800 | bytes 10158080 | tf_op jit(solution)/shard_map/dot_general | solution.py:297
  144.6 1.4 fusion.13
  146.0 8.4 %all_gather.3 = bf16[192,2048]{1,0:T(8,128)(2,1)S(1)} all-gather(bf16[192,512]{1,0:T(8,128)(2,1)S(1)} %fusion.13), channel_id=1, replica_groups=mesh['sp'=8,'tp'=4] {'tp'}, dimensions={1}, use_global_device_ids=true | all-gather | bytes 983040 | tf_op jit(solution)/shard_map/all_gather | solution.py:409
  154.4 1.5 convolution_convert_fusion
  155.9 1.1 fusion.58
  157.1 31.4 %tail.1 = (f32[192,256]{1,0:T(8,128)}, f32[256,256]{1,0:T(8,128)}) custom-call(f32[192,256]{1,0:T(8,128)} %exp.22.decay_ref, f32[192,256]{1,0:T(8,128)} %get-tuple-element.27.input_ref, bf16[8,256,256]{2,1,0:T(8,128)(2,1)} %bitcast.135), custom_call_target="tpu_custom_call" | custom-call | tf_op jit(solution)/shard_map/tail/pallas_call | solution.py:260
  188.5 1.2 fusion.64
  189.7 1.0 fusion.67
  190.8 1.0 fusion.14
  191.8 1.7 bitcast_add_fusion
  (55 shorter events, 5.2 us)
Async XLA Ops:
  7.2 148.7 %copy-start = (bf16[2048,256]{1,0:T(8,128)(2,1)S(1)}, bf16[2048,256]{1,0:T(8,128)(2,1)}, u32[]{:S(2)}) copy-start(bf16[2048,256]{1,0:T(8,128)(2,1)} %param.21) | copy-start | bytes 3145732
  7.2 5.4 %copy-start.4 = (bf16[192,256]{1,0:T(8,128)(2,1)S(1)}, bf16[192,256]{1,0:T(8,128)(2,1)}, u32[]{:S(2)}) copy-start(bf16[192,256]{1,0:T(8,128)(2,1)} %param.22) | copy-start | bytes 294916
  7.2 6.4 %copy-start.10 = (f32[256]{0:T(256)S(1)}, f32[256]{0:T(256)}, u32[]{:S(2)}) copy-start(f32[256]{0:T(256)} %param.26) | copy-start | bytes 3076
  7.2 6.4 %copy-start.6 = (f32[192,256]{1,0:T(8,128)S(1)}, f32[192,256]{1,0:T(8,128)}, u32[]{:S(2)}) copy-start(f32[192,256]{1,0:T(8,128)} %param.27) | copy-start | bytes 589828
  7.2 110.5 %reduce-scatter.2.cloned.1.call-start = ((), (), s32[]{:S(2)}) async-start(), calls=%async_computation.2 | async-start | bytes 2949120 | tf_op jit(solution)/shard_map/reduce_scatter | solution.py:398
  9.2 6.0 %copy-start.9 = (f32[192,2]{0,1:T(2,128)S(1)}, f32[192,2]{0,1:T(2,128)}, u32[]{:S(2)}) copy-start(f32[192,2]{0,1:T(2,128)} %param.17) | copy-start | bytes 4612
  11.4 3.9 %copy-start.8 = (pred[1,8,72,192]{3,2,1,0:T(8,128)(4,1)S(1)}, pred[1,8,72,192]{3,2,1,0:T(8,128)(4,1)}, u32[]{:S(2)}) copy-start(pred[1,8,72,192]{3,2,1,0:T(8,128)(4,1)} %get-tuple-element.29) | copy-start | bytes 331780
  59.8 3.5 %copy-start.12 = (bf16[1,2048,896]{2,1,0:T(8,128)(2,1)S(1)}, bf16[1,2048,896]{2,1,0:T(8,128)(2,1)}, u32[]{:S(2)}) copy-start(bf16[1,2048,896]{2,1,0:T(8,128)(2,1)} %param.18) | copy-start | bytes 11010052
  62.7 3.1 %copy-start.3 = (bf16[1,8,72,2048]{3,2,1,0:T(8,128)(2,1)}, bf16[1,8,72,2048]{3,2,1,0:T(8,128)(2,1)S(1)}, u32[]{:S(2)}) copy-start(bf16[1,8,72,2048]{3,2,1,0:T(8,128)(2,1)S(1)} %get-tuple-element.21) | copy-start | bytes 7077892
  62.7 6.3 %copy-start.1 = (bf16[1,8,72,2048]{3,2,1,0:T(8,128)(2,1)}, bf16[1,8,72,2048]{3,2,1,0:T(8,128)(2,1)S(1)}, u32[]{:S(2)}) copy-start(bf16[1,8,72,2048]{3,2,1,0:T(8,128)(2,1)S(1)} %get-tuple-element.20) | copy-start | bytes 7077892
  63.2 3.2 %copy-start.13 = (bf16[1,2048,896]{2,1,0:T(8,128)(2,1)S(1)}, bf16[1,2048,896]{2,1,0:T(8,128)(2,1)}, u32[]{:S(2)}) copy-start(bf16[1,2048,896]{2,1,0:T(8,128)(2,1)} %param.19) | copy-start | bytes 11010052
  66.4 2.6 %copy-start.17 = (f32[576,896]{1,0:T(8,128)}, f32[576,896]{1,0:T(8,128)S(1)}, u32[]{:S(2)}) copy-start(f32[576,896]{1,0:T(8,128)S(1)} %fusion.2) | copy-start | bytes 6193156
  66.4 2.8 %copy-start.11 = (bf16[1,896,2048]{2,1,0:T(8,128)(2,1)S(1)}, bf16[1,896,2048]{2,1,0:T(8,128)(2,1)}, u32[]{:S(2)}) copy-start(bf16[1,896,2048]{2,1,0:T(8,128)(2,1)} %param.20) | copy-start | bytes 11010052
  69.0 3.4 %copy-start.19 = (f32[576,896]{1,0:T(8,128)}, f32[576,896]{1,0:T(8,128)S(1)}, u32[]{:S(2)}) copy-start(f32[576,896]{1,0:T(8,128)S(1)} %fusion.6) | copy-start | bytes 6193156
  72.4 2.7 %copy-start.16 = (bf16[576,896]{1,0:T(8,128)(2,1)}, bf16[576,896]{1,0:T(8,128)(2,1)S(1)}, u32[]{:S(2)}) copy-start(bf16[576,896]{1,0:T(8,128)(2,1)S(1)} %get-tuple-element.23) | copy-start | bytes 3096580
  125.5 18.5 %all-to-all-start = ((bf16[8,2,18432]{2,1,0:T(2,128)(2,1)}), bf16[8,2,18432]{2,1,0:T(2,128)(2,1)S(1)}, u32[]{:S(2)}, u32[]{:S(2)}) async-start(bf16[8,2,18432]{2,1,0:T(2,128)(2,1)} %reshape.131), calls=%async_computation.1 | async-start | bytes 1179648 | tf_op jit(solution)/shard_map/all_to_all | solution.py:401
  131.6 7.3 %copy-start.2 = (bf16[1,8,72,2048]{3,2,1,0:T(8,128)(2,1)S(1)}, bf16[1,8,72,2048]{3,2,1,0:T(8,128)(2,1)}, u32[]{:S(2)}) copy-start(bf16[1,8,72,2048]{3,2,1,0:T(8,128)(2,1)} %copy-done.1) | copy-start | bytes 7077892
  131.6 7.3 %copy-start.18 = (f32[576,896]{1,0:T(8,128)S(1)}, f32[576,896]{1,0:T(8,128)}, u32[]{:S(2)}) copy-start(f32[576,896]{1,0:T(8,128)} %copy-done.17) | copy-start | bytes 6193156
  131.6 7.3 %copy-start.20 = (f32[576,896]{1,0:T(8,128)S(1)}, f32[576,896]{1,0:T(8,128)}, u32[]{:S(2)}) copy-start(f32[576,896]{1,0:T(8,128)} %copy-done.19) | copy-start | bytes 6193156
  144.6 9.8 %copy-start.14 = (f32[192,256]{1,0:T(8,128)S(1)}, f32[192,256]{1,0:T(8,128)}, u32[]{:S(2)}) copy-start(f32[192,256]{1,0:T(8,128)} %get-tuple-element.12) | copy-start | bytes 589828
  144.6 9.8 %copy-start.15 = (bf16[192,256]{1,0:T(8,128)(2,1)S(1)}, bf16[192,256]{1,0:T(8,128)(2,1)}, u32[]{:S(2)}) copy-start(bf16[192,256]{1,0:T(8,128)(2,1)} %param.23) | copy-start | bytes 294916
  155.9 32.6 %copy-start.7 = (f32[192,256]{1,0:T(8,128)S(1)}, f32[192,256]{1,0:T(8,128)}, u32[]{:S(2)}) copy-start(f32[192,256]{1,0:T(8,128)} %get-tuple-element.15) | copy-start | bytes 589828
  188.5 5.1 %copy-start.5 = (f32[256,256]{1,0:T(8,128)S(1)}, f32[256,256]{1,0:T(8,128)}, u32[]{:S(2)}) copy-start(f32[256,256]{1,0:T(8,128)} %get-tuple-element.41) | copy-start | bytes 786436
Sparse Core Ops, SparseCore 0:
  79.2 38.4 reduce-scatter.1
where the time goes:
time: 202 us; the launch traced here: 201 us
  Pallas kernels  74.2 us (37%)
  matrix products  43.9 us (22%)
  waiting for transfers between devices  32.3 us (16%)
  between operations  14.4 us (7%)
  other arithmetic  11.1 us (5%)
  local copies, waits for them, and re-layouts  10.6 us (5%)
  blocking collectives  8.38 us (4%)
  starting transfers between devices  6.1 us (3%)
    pallas_call x1, Pallas kernels, dispatch(): pl.pallas_call(functools.partial(dispatch_kernel, n, m), out_shape=(jax.S...  42.8 us
    reduce_scatter x1, waiting for transfers between devices, per_device(): lax.psum_scatter(partial_value.astype(jnp.bfloat16), 'tp', scatter_dimens...  31.8 us
    pallas_call x1, Pallas kernels, tail(): pl.pallas_call(functools.partial(tail_kernel, n), out_shape=(jax.ShapeDty...  31.4 us
    all_gather x1, blocking collectives, per_device(): grad_full = lax.all_gather(residual_grad, 'tp', axis=1, tiled=True)  8.38 us
    dot_general x1, matrix products, expert_backward(): lax.dot_general(inputs, d_gate, (((0,), (0,)), ((), ())), preferred_eleme...  7.28 us
    dot_general x1, matrix products, expert_backward(): lax.dot_general(inputs, d_up, (((0,), (0,)), ((), ())), preferred_element...  6.86 us
    all_to_all x1, starting transfers between devices, per_device(): lax.all_to_all(slot_grad[None], 'sp', split_axis=1, concat_axis=0, tiled=...  6.06 us
    unnamed x2, other arithmetic  5.46 us
  transfers between devices with their start and end apart: 2, of which 2 were waited for; matrix products, arithmetic and copies ran while one was open for 9% of the time, Pallas kernels for 0%

commit v1 on v0

--- a/solution.py
+++ b/solution.py
@@ -58,10 +58,12 @@
 def dispatch_kernel(
     n,
     m,
-    send_ref,
+    rows_ref,
+    cot_ref,
     decay_ref,
     driven_ref,
-    out_ref,
+    rows_out,
+    cot_out,
     states_ref,
     prev_ref,
     gain_buf,
@@ -75,38 +77,45 @@
     car_rsem,
     self_sem,
 ):
+    sources, targets = (rows_ref, cot_ref), (rows_out, cot_out)
     s, t = lax.axis_index("sp"), lax.axis_index("tp")
-    feat = send_ref.shape[3]
+    feat = rows_ref.shape[2]
     stages = m.bit_length() - 1
     greet(
         [{"sp": lax.rem(s + k, n)} for k in range(1, n)]
         + [{"tp": partner(t, j, m)} for j in range(stages)]
     )
 
-    def block(src, col):
-        return out_ref.at[:, src, :, pl.ds(pl.multiple_of(col * feat, feat), feat)]
+    def block(a, src, col):
+        return targets[a].at[src, :, pl.ds(pl.multiple_of(col * feat, feat), feat)]
 
     first = []
-    own = pltpu.make_async_copy(send_ref.at[:, s], block(s, t), self_sem)
-    own.start()
-    for k in range(1, n):
+    for k in range(n):
         dst = lax.rem(s + k, n)
-        copy = remote(
-            send_ref.at[:, dst], block(s, t), a2a_send.at[k], a2a_recv.at[k], {"sp": dst}
-        )
-        copy.start()
-        first.append(copy)
+        for a in range(2):
+            if k == 0:
+                copy = pltpu.make_async_copy(sources[a].at[s], block(a, s, t), self_sem.at[a])
+            else:
+                copy = remote(
+                    sources[a].at[dst],
+                    block(a, s, t),
+                    a2a_send.at[a, k],
+                    a2a_recv.at[a, k],
+                    {"sp": dst},
+                )
+            copy.start()
+            first.append(copy)
 
     pushed = []
 
-    def push(k, stage, i, col):
+    def push(a, k, stage, i, col):
         src = lax.rem(s + n - k, n)
         at = 2**stage - 1 + i
         copy = remote(
-            block(src, col),
-            block(src, col),
-            tp_send.at[at, k],
-            tp_recv.at[at, k],
+            block(a, src, col),
+            block(a, src, col),
+            tp_send.at[a, at, k],
+            tp_recv.at[a, at, k],
             {"tp": partner(t, stage, m)},
         )
         copy.start()
@@ -117,23 +126,25 @@
         cols = held_columns(partner(t, stage, m), stage, m)
         for i, col in enumerate(cols):
             at = 2**stage - 1 + i
-            remote(
-                block(src, col),
-                block(src, col),
-                tp_send.at[at, k],
-                tp_recv.at[at, k],
-                {"tp": partner(t, stage, m)},
-            ).wait_recv()
-            for later in range(stage + 1, stages):
-                push(k, later, 2**stage + i, col)
+            for a in range(2):
+                remote(
+                    block(a, src, col),
+                    block(a, src, col),
+                    tp_send.at[a, at, k],
+                    tp_recv.at[a, at, k],
+                    {"tp": partner(t, stage, m)},
+                ).wait_recv()
+                for later in range(stage + 1, stages):
+                    push(a, k, later, 2**stage + i, col)
 
     def forward(k):
-        if k == 0:
-            own.wait()
-        else:
-            first[k - 1].wait_recv()
-        for stage in range(stages):
-            push(k, stage, 0, t)
+        for a in range(2):
+            if k == 0:
+                first[a].wait()
+            else:
+                first[2 * k + a].wait_recv()
+            for stage in range(stages):
+                push(a, k, stage, 0, t)
 
     forward(0)
     gain, term = local_scan(decay_ref[...], driven_ref[...], False)
@@ -167,38 +178,211 @@
             arrived(k, stage)
     for k in range(n):
         arrived(k, stages - 1)
-    for copy in first:
+    for copy in first[2:]:
         copy.wait_send()
     for copy in pushed:
         copy.wait_send()
 
 
-def dispatch(send, decay, driven):
+def dispatch(send_rows, send_cot, decay, driven):
     n, m = lax.axis_size("sp"), lax.axis_size("tp")
-    two, _, cap, feat = send.shape
+    _, cap, feat = send_rows.shape
+    whole = jax.ShapeDtypeStruct((n, cap, m * feat), send_rows.dtype)
     rows, channels = decay.shape
     vmem = pl.BlockSpec(memory_space=pltpu.VMEM)
     state = jax.ShapeDtypeStruct((rows, channels), jnp.float32)
     return pl.pallas_call(
         functools.partial(dispatch_kernel, n, m),
-        out_shape=(jax.ShapeDtypeStruct((two, n, cap, m * feat), send.dtype), state, state),
-        in_specs=[vmem] * 3,
-        out_specs=(vmem,) * 3,
+        out_shape=(whole, whole, state, state),
+        in_specs=[vmem] * 4,
+        out_specs=(vmem,) * 4,
         scratch_shapes=[
             pltpu.VMEM((rows, channels), jnp.float32),
             pltpu.VMEM((2, channels), jnp.float32),
             pltpu.VMEM((n, 2, channels), jnp.float32),
-            pltpu.SemaphoreType.DMA((n,)),
-            pltpu.SemaphoreType.DMA((n,)),
-            pltpu.SemaphoreType.DMA((m - 1, n)),
-            pltpu.SemaphoreType.DMA((m - 1, n)),
-            pltpu.SemaphoreType.DMA((n,)),
-            pltpu.SemaphoreType.DMA((n,)),
-            pltpu.SemaphoreType.DMA,
+            pltpu.SemaphoreType.DMA((2, n)),
+            pltpu.SemaphoreType.DMA((2, n)),
+            pltpu.SemaphoreType.DMA((2, m - 1, n)),
+            pltpu.SemaphoreType.DMA((2, m - 1, n)),
+            pltpu.SemaphoreType.DMA((n,)),
+            pltpu.SemaphoreType.DMA((n,)),
+            pltpu.SemaphoreType.DMA((2,)),
         ],
         compiler_params=pltpu.CompilerParams(collective_id=0, has_side_effects=True),
         name="dispatch",
-    )(send, decay, driven)
+    )(send_rows, send_cot, decay, driven)
+
+
+def return_kernel(
+    n,
+    m,
+    part_ref,
+    pick_ref,
+    cot_ref,
+    out_ref,
+    in_buf,
+    acc_buf,
+    back_buf,
+    rs_send,
+    rs_recv,
+    a2a_send,
+    a2a_recv,
+    ag_send,
+    ag_recv,
+):
+    s, t = lax.axis_index("sp"), lax.axis_index("tp")
+    feat = cot_ref.shape[1]
+    stages = m.bit_length() - 1
+
+    def across(stage):
+        d = 2**stage
+        return t + d * (1 - 2 * ((t // d) % 2))
+
+    greet(
+        [{"sp": lax.rem(s + k, n)} for k in range(1, n)] + [{"tp": across(j)} for j in range(stages)]
+    )
+
+    def cols(col):
+        return pl.ds(pl.multiple_of(col * feat, feat), feat)
+
+    base = []
+    total = 0
+    for stage in range(stages):
+        base.append(total)
+        total += m >> (stage + 1)
+
+    order = list(range(1, n)) + [0]
+    waits = []
+
+    def send_stage(k, stage):
+        dst = lax.rem(s + k, n)
+        source = part_ref if stage == 0 else acc_buf
+        peer = across(stage)
+        step = 2 ** (stage + 1)
+        for i in range(m // step):
+            col = lax.rem(peer + i * step, m)
+            at = base[stage] + i
+            copy = remote(
+                source.at[dst, :, cols(col)],
+                in_buf.at[at, k],
+                rs_send.at[at, k],
+                rs_recv.at[at, k],
+                {"tp": peer},
+            )
+            copy.start()
+            waits.append(copy)
+
+    def sum_stage(k, stage):
+        dst = lax.rem(s + k, n)
+        source = part_ref if stage == 0 else acc_buf
+        step = 2 ** (stage + 1)
+        for i in range(m // step):
+            col = lax.rem(t + i * step, m)
+            at = base[stage] + i
+            remote(
+                source.at[dst, :, cols(col)],
+                in_buf.at[at, k],
+                rs_send.at[at, k],
+                rs_recv.at[at, k],
+                {"tp": across(stage)},
+            ).wait_recv()
+            mine = source[dst, :, cols(col)].astype(jnp.float32)
+            acc_buf[dst, :, cols(col)] = (mine + in_buf[at, k].astype(jnp.float32)).astype(
+                jnp.bfloat16
+            )
+
+    def send_home(k):
+        dst = lax.rem(s + k, n)
+        if k == 0:
+            back_buf[s] = acc_buf[s, :, cols(t)]
+            return
+        copy = remote(
+            acc_buf.at[dst, :, cols(t)],
+            back_buf.at[s],
+            a2a_send.at[k],
+            a2a_recv.at[k],
+            {"sp": dst},
+        )
+        copy.start()
+        waits.append(copy)
+
+    for k in order:
+        send_stage(k, 0)
+    for at in range(n + stages - 1):
+        for stage in range(stages):
+            if 0 <= at - stage < n:
+                k = order[at - stage]
+                sum_stage(k, stage)
+                if stage + 1 < stages:
+                    send_stage(k, stage + 1)
+                else:
+                    send_home(k)
+    value = cot_ref[...].astype(jnp.float32)
+    for k in range(n):
+        src = lax.rem(s + n - k, n)
+        if k > 0:
+            remote(
+                acc_buf.at[src, :, cols(t)],
+                back_buf.at[src],
+                a2a_send.at[k],
+                a2a_recv.at[k],
+                {"sp": src},
+            ).wait_recv()
+        value = value + jnp.dot(
+            pick_ref[src], back_buf[src], preferred_element_type=jnp.float32
+        )
+    out_ref[:, cols(t)] = value.astype(jnp.bfloat16)
+
+    def share(stage, i, col):
+        at = 2**stage - 1 + i
+        return remote(
+            out_ref.at[:, cols(col)],
+            out_ref.at[:, cols(col)],
+            ag_send.at[at],
+            ag_recv.at[at],
+            {"tp": partner(t, stage, m)},
+        )
+
+    def push(stage, i, col):
+        copy = share(stage, i, col)
+        copy.start()
+        waits.append(copy)
+
+    for stage in range(stages):
+        push(stage, 0, t)
+    for stage in range(stages):
+        for i, col in enumerate(held_columns(partner(t, stage, m), stage, m)):
+            share(stage, i, col).wait_recv()
+            for later in range(stage + 1, stages):
+                push(later, 2**stage + i, col)
+    for copy in waits:
+        copy.wait_send()
+
+
+def bring_back(part, pick, output_gradient):
+    n, m = lax.axis_size("sp"), lax.axis_size("tp")
+    _, cap, width = part.shape
+    rows, feat = output_gradient.shape
+    vmem = pl.BlockSpec(memory_space=pltpu.VMEM)
+    return pl.pallas_call(
+        functools.partial(return_kernel, n, m),
+        out_shape=jax.ShapeDtypeStruct((rows, width), jnp.bfloat16),
+        in_specs=[vmem] * 3,
+        out_specs=vmem,
+        scratch_shapes=[
+            pltpu.VMEM((m - 1, n, cap, feat), jnp.bfloat16),
+            pltpu.VMEM((n, cap, width), jnp.bfloat16),
+            pltpu.VMEM((n, cap, feat), jnp.bfloat16),
+            pltpu.SemaphoreType.DMA((m - 1, n)),
+            pltpu.SemaphoreType.DMA((m - 1, n)),
+            pltpu.SemaphoreType.DMA((n,)),
+            pltpu.SemaphoreType.DMA((n,)),
+            pltpu.SemaphoreType.DMA((m - 1,)),
+            pltpu.SemaphoreType.DMA((m - 1,)),
+        ],
+        compiler_params=pltpu.CompilerParams(collective_id=2, has_side_effects=True),
+        name="bring_back",
+    )(part, pick, output_gradient)
 
 
 def tail_kernel(
@@ -364,7 +548,6 @@
     pair_cot = pair_cot.reshape(-1, feat_width)
     send_rows = jnp.dot(pick_any, middle_stream, preferred_element_type=jnp.bfloat16)
     send_cot = jnp.dot(pick_both, pair_cot, preferred_element_type=jnp.bfloat16)
-    send = jnp.stack([send_rows, send_cot]).reshape(2, experts, capacity, feat_width)
     channels = recurrence_input.shape[1]
     block_width = recurrence_gate_weight.shape[1]
     local_blocks = channels // block_width
@@ -388,25 +571,23 @@
     input_scale = jnp.sqrt(-jnp.expm1(2.0 * decay_logarithm))
     u_float = recurrence_input.astype(jnp.float32)
     driven = u_float * admit_gate * input_scale
-    received, states, prev_states = dispatch(send, decay_step, driven)
-    row_width = received.shape[3]
-    inputs = received[0].reshape(-1, row_width)
-    cotangent = received[1].reshape(-1, row_width)
+    recv_rows, recv_cot, states, prev_states = dispatch(
+        send_rows.reshape(experts, capacity, feat_width),
+        send_cot.reshape(experts, capacity, feat_width),
+        decay_step,
+        driven,
+    )
+    row_width = recv_rows.shape[2]
+    inputs = recv_rows.reshape(-1, row_width)
+    cotangent = recv_cot.reshape(-1, row_width)
     grad_gate, grad_up, grad_down, partial_value = expert_backward(
         inputs, cotangent, expert_gate_weight[0], expert_up_weight[0], expert_down_weight[0]
     )
-    slot_grad = lax.psum_scatter(
-        partial_value.astype(jnp.bfloat16), "tp", scatter_dimension=1, tiled=True
-    )
-    returned = lax.all_to_all(slot_grad[None], "sp", split_axis=1, concat_axis=0, tiled=True)
-    arrived = lax.dot_general(
-        pick_any,
-        returned.reshape(experts * capacity, -1),
-        (((0,), (0,)), ((), ())),
-        preferred_element_type=jnp.float32,
-    )
-    residual_grad = (output_gradient.astype(jnp.float32) + arrived).astype(jnp.bfloat16)
-    grad_full = lax.all_gather(residual_grad, "tp", axis=1, tiled=True)
+    grad_full = bring_back(
+        partial_value.astype(jnp.bfloat16).reshape(experts, capacity, row_width),
+        pick_any.reshape(experts, capacity, rows_dev).transpose(0, 2, 1),
+        output_gradient,
+    )
     mixer_grad = jnp.dot(grad_full, recurrent_output_weight, preferred_element_type=jnp.float32)
     gelu_val, gelu_der = gelu_parts(output_gate_logits)
     lru_out = (states * gelu_val).astype(jnp.bfloat16)

time: 202 us -> 170 us (0.84)
  Pallas kernels: 74.2 us -> 112 us
  waiting for transfers between devices: 32.3 us -> 0 us
  between operations: 14.4 us -> 0.96 us
  blocking collectives: 8.38 us -> 0 us
  local copies, waits for them, and re-layouts: 10.6 us -> 2.47 us
  starting transfers between devices: 6.1 us -> 0 us
  other arithmetic: 11.1 us -> 7.01 us
  matrix products: 43.9 us -> 46.5 us
    pallas_call x1 -> x2, Pallas kernels: 42.8 us -> 82.5 us  [the longest x1 42.4 us: dispatch(): pl.pallas_call(functools.partial(dispatch_kernel, n, m), out_shape=(whole...]
    reduce_scatter x1 -> x0, waiting for transfers between devices: 31.8 us -> none  [per_device(): lax.psum_scatter(partial_value.astype(jnp.bfloat16), 'tp', scatter_dimens...]
    all_gather x1 -> x0, blocking collectives: 8.38 us -> none  [per_device(): grad_full = lax.all_gather(residual_grad, 'tp', axis=1, tiled=True)]
    all_to_all x1 -> x0, starting transfers between devices: 6.06 us -> none  [per_device(): lax.all_to_all(slot_grad[None], 'sp', split_axis=1, concat_axis=0, tiled=...]
    unnamed x2 -> x1, other arithmetic: 5.46 us -> 1.35 us
    slice x1 -> x0, local copies, waits for them, and re-layouts: 2.92 us -> none  [per_device(): cotangent = received[1].reshape(-1, row_width)]
    dot_general x1, matrix products: 2.6 us -> 5.49 us  [expert_backward(): gate_act = jnp.dot(inputs, gate_weight, preferred_element_type=jnp.float32)]
    unnamed x46 -> x43, local copies, waits for them, and re-layouts: 4.21 us -> 1.67 us
  transfers between devices with their start and end apart: 2 -> 0, of which waited for: 2 -> 0; matrix products, arithmetic and copies ran while one was open for 9% -> 0% of each run, Pallas kernels for 0% -> 0%
where the time goes in v1:
time: 170 us; the launch traced here: 169 us
  Pallas kernels  112 us (66%)
  matrix products  46.5 us (27%)
  other arithmetic  7.01 us (4%)
  local copies, waits for them, and re-layouts  2.47 us (1%)
    pallas_call x1, Pallas kernels, dispatch(): pl.pallas_call(functools.partial(dispatch_kernel, n, m), out_shape=(whole...  42.4 us
    pallas_call x1, Pallas kernels, bring_back(): pl.pallas_call(functools.partial(return_kernel, n, m), out_shape=jax.Shap...  40 us
    pallas_call x1, Pallas kernels, tail(): pl.pallas_call(functools.partial(tail_kernel, n), out_shape=(jax.ShapeDty...  29.7 us
    dot_general x1, matrix products, expert_backward(): lax.dot_general(hidden, cotangent, (((0,), (0,)), ((), ())), preferred_el...  7.02 us
    dot_general x1, matrix products, expert_backward(): gate_act = jnp.dot(inputs, gate_weight, preferred_element_type=jnp.float32)  5.49 us
    dot_general x1, matrix products, expert_backward(): lax.dot_general(inputs, d_up, (((0,), (0,)), ((), ())), preferred_element...  4.84 us
    dot_general x1, matrix products, expert_backward(): lax.dot_general(inputs, d_gate, (((0,), (0,)), ((), ())), preferred_eleme...  4.84 us
    dot_general x1, matrix products, expert_backward(): lax.dot_general(d_up, up_weight, (((1,), (1,)), ((), ())), preferred_elem...  3.89 us

profile of v1, /device:TPU:12, one launch (start us, length us, event | category | flops | bytes accessed | tf_op | source)
XLA Modules:
  0.0 169.0 jit_solution(7683702054697495537)
XLA Ops:
  0.7 1.2 fusion.17
  1.9 1.1 fusion.21
  3.0 0.7 fusion.90
  3.7 1.8 %fusion.63 = (f32[192,256]{1,0:T(8,128)}, f32[192,256]{1,0:T(8,128)S(1)}) fusion(f32[2,24,8,128]{3,2,1,0:T(8,128)S(1)} %fusion.17, bf16[192,256]{1,0:T(8,128)(2,1)} %param.22, f32[192,256]{1,0:T(8,128)} %param.27, f32[256]{0:T(256)S(1)} %fusion.90, f32[2,24,8,128]{3,2,1,0:T(8,128)S(1)} %fusion.21), kind=kLoop, calls=%fused_computation.94 | loop fusion | flops 344064 | bytes 1082368 | tf_op jit(solution)/shard_map/mul | solution.py:573
  5.5 0.7 exp.22.decay_ref
  6.2 0.2 select_reduce_fusion.1
  6.4 0.2 broadcast_compare_fusion.1
  6.7 0.1 mul.170
  6.8 0.1 fusion.27
  6.9 1.3 fusion.23.cot_ref
  8.3 1.1 fusion.34
  9.4 42.4 %dispatch.1 = (bf16[8,72,2048]{2,1,0:T(8,128)(2,1)}, bf16[8,72,2048]{2,1,0:T(8,128)(2,1)}, f32[192,256]{1,0:T(8,128)}, f32[192,256]{1,0:T(8,128)}) custom-call(bf16[8,72,512]{2,1,0:T(8,128)(2,1)} %bitcast.120, bf16[8,72,512]{2,1,0:T(8,128)(2,1)} %fusion.23.cot_ref, f32[192,256]{1,0:T(8,128)} %exp.22.decay_ref, f32[192,256]{1,0:T(8,128)} %get-tuple-element.20.driven_ref), custom_call_target="tpu_custom_call" | custom-call | tf_op jit(solution)/shard_map/dispatch/pallas_call | solution.py:194
  51.9 5.5 %fusion.2 = f32[576,896]{1,0:T(8,128)S(1)} fusion(bf16[576,2048]{1,0:T(8,128)(2,1)} %bitcast.125, bf16[1,2048,896]{2,1,0:T(8,128)(2,1)} %param.18), kind=kOutput, calls=%fused_computation.3 | convolution fusion | flops 2113929216 | bytes 8093696 | tf_op jit(solution)/shard_map/dot_general | solution.py:473
  57.4 2.6 %fusion.6 = f32[576,896]{1,0:T(8,128)S(1)} fusion(bf16[576,2048]{1,0:T(8,128)(2,1)S(1)} %bitcast.126, bf16[1,2048,896]{2,1,0:T(8,128)(2,1)S(1)} %copy-done.9), kind=kOutput, calls=%fused_computation.7 | convolution fusion | flops 2113929216 | bytes 8093696 | tf_op jit(solution)/shard_map/dot_general | solution.py:474
  60.1 0.1 copy-done.7
  60.2 0.7 copy-done.12
  60.9 3.2 %multiply_convert_fusion.1 = (bf16[576,896]{1,0:T(8,128)(2,1)S(1)}, bf16[576,896]{1,0:T(8,128)(2,1)S(1)}) fusion(f32[576,896]{1,0:T(8,128)S(1)} %fusion.2, f32[576,896]{1,0:T(8,128)S(1)} %fusion.6, bf16[576,2048]{1,0:T(8,128)(2,1)S(1)} %bitcast.129, bf16[1,896,2048]{2,1,0:T(8,128)(2,1)S(1)} %copy-done.7), kind=kOutput, calls=%fused_computation.16 | convolution fusion | flops 2120638464 | bytes 12222464 | tf_op jit(solution)/shard_map/dot_general | solution.py:478
  64.2 2.6 %fusion = f32[576,2048]{1,0:T(8,128)S(1)} fusion(bf16[576,896]{1,0:T(8,128)(2,1)S(1)} %get-tuple-element.23, bf16[1,2048,896]{2,1,0:T(8,128)(2,1)S(1)} %copy-done.8), kind=kOutput, calls=%fused_computation.1 | convolution fusion | flops 2113929216 | bytes 9420800 | tf_op jit(solution)/shard_map/dot_general | solution.py:494
  66.9 3.9 %add_convert_fusion = bf16[576,2048]{1,0:T(8,128)(2,1)} fusion(f32[576,2048]{1,0:T(8,128)S(1)} %fusion, bf16[576,896]{1,0:T(8,128)(2,1)S(1)} %get-tuple-element.22, bf16[1,2048,896]{2,1,0:T(8,128)(2,1)S(1)} %copy-done.9), kind=kOutput, calls=%fused_computation | convolution fusion | flops 2116288512 | bytes 11780096 | tf_op jit(solution)/shard_map/dot_general | solution.py:497
  70.8 1.0 fusion.30.pick_ref
  71.7 40.0 %bring_back.1 = bf16[192,2048]{1,0:T(8,128)(2,1)} custom-call(bf16[8,72,2048]{2,1,0:T(8,128)(2,1)} %bitcast.118, bf16[8,192,72]{2,1,0:T(8,128)(2,1)} %fusion.30.pick_ref, bf16[192,512]{1,0:T(8,128)(2,1)} %cot_ref.1), custom_call_target="tpu_custom_call" | custom-call | tf_op jit(solution)/shard_map/bring_back/pallas_call | solution.py:367
  111.8 2.6 %convolution_convert_fusion = bf16[2048,256]{1,0:T(8,128)(2,1)} fusion(bf16[192,2048]{1,0:T(8,128)(2,1)} %bring_back.1, f32[192,256]{1,0:T(8,128)S(1)} %copy-done.15, bf16[192,256]{1,0:T(8,128)(2,1)S(1)} %copy-done.16), kind=kOutput, calls=%fused_computation.14 | convolution fusion | flops 202391552 | bytes 2129920 | tf_op jit(solution)/shard_map/dot_general | solution.py:594
  114.5 2.3 %fusion.58 = (f32[192,256]{1,0:T(8,128)}, f32[192,256]{1,0:T(8,128)}) fusion(bf16[192,256]{1,0:T(8,128)(2,1)S(1)} %copy-done.16, f32[192,256]{1,0:T(8,128)S(1)} %copy-done.15, bf16[192,2048]{1,0:T(8,128)(2,1)} %bring_back.1, bf16[2048,256]{1,0:T(8,128)(2,1)S(1)} %copy-done), kind=kOutput, calls=%fused_computation.81 | convolution fusion | flops 202358784 | bytes 2523136 | tf_op jit(solution)/shard_map/dot_general | solution.py:591
  116.8 29.7 %tail.1 = (f32[192,256]{1,0:T(8,128)}, f32[256,256]{1,0:T(8,128)}) custom-call(f32[192,256]{1,0:T(8,128)} %exp.22.decay_ref, f32[192,256]{1,0:T(8,128)} %get-tuple-element.27.input_ref, bf16[8,256,256]{2,1,0:T(8,128)(2,1)} %bitcast.119), custom_call_target="tpu_custom_call" | custom-call | tf_op jit(solution)/shard_map/tail/pallas_call | solution.py:444
  146.5 1.3 fusion.64
  147.8 1.0 fusion.67
  148.8 1.0 fusion.13
  149.9 1.7 %bitcast_add_fusion = f32[192,256]{1,0:T(8,128)} fusion(f32[2,24,8,128]{3,2,1,0:T(8,128)S(1)} %fusion.13, f32[192,256]{1,0:T(8,128)} %get-tuple-element.16, f32[2,24,8,128]{3,2,1,0:T(8,128)S(1)} %fusion.17, f32[192,256]{1,0:T(8,128)S(1)} %get-tuple-element.21), kind=kLoop, calls=%fused_computation.82 | loop fusion | flops 245760 | bytes 983040 | tf_op jit(solution)/shard_map/add | solution.py:622
  151.6 7.0 %convert_bitcast_fusion = bf16[1,896,2048]{2,1,0:T(8,128)(2,1)} fusion(bf16[576,2048]{1,0:T(8,128)(2,1)S(1)} %bitcast.130, f32[576,896]{1,0:T(8,128)} %copy-done.18, f32[576,896]{1,0:T(8,128)} %copy-done.17), kind=kOutput, calls=%fused_computation.11 | convolution fusion | flops 2118860800 | bytes 10158080 | tf_op jit(solution)/shard_map/dot_general | solution.py:481
  158.6 4.8 %convert_bitcast_fusion.1 = bf16[1,2048,896]{2,1,0:T(8,128)(2,1)} fusion(bf16[576,2048]{1,0:T(8,128)(2,1)S(1)} %bitcast.127, bf16[576,896]{1,0:T(8,128)(2,1)S(1)} %copy-done.20), kind=kOutput, calls=%fused_computation.12 | convolution fusion | flops 2115764224 | bytes 7061504 | tf_op jit(solution)/shard_map/dot_general | solution.py:491
  163.5 4.8 %convert_bitcast_fusion.2 = bf16[1,2048,896]{2,1,0:T(8,128)(2,1)} fusion(bf16[576,2048]{1,0:T(8,128)(2,1)S(1)} %bitcast.128, bf16[576,896]{1,0:T(8,128)(2,1)S(1)} %get-tuple-element.23), kind=kOutput, calls=%fused_computation.13 | convolution fusion | flops 2115764224 | bytes 7061504 | tf_op jit(solution)/shard_map/dot_general | solution.py:488
  168.3 0.7 copy.67
  (44 shorter events, 0.1 us)
Async XLA Ops:
  0.6 113.8 %copy-start = (bf16[2048,256]{1,0:T(8,128)(2,1)S(1)}, bf16[2048,256]{1,0:T(8,128)(2,1)}, u32[]{:S(2)}) copy-start(bf16[2048,256]{1,0:T(8,128)(2,1)} %param.21) | copy-start | bytes 3145732
  0.6 5.6 %copy-start.5 = (s32[192,2]{0,1:T(2,128)S(1)}, s32[192,2]{0,1:T(2,128)}, u32[]{:S(2)}) copy-start(s32[192,2]{0,1:T(2,128)} %param.16) | copy-start | bytes 4612
  0.7 6.0 %copy-start.1 = (bf16[192,512]{1,0:T(8,128)(2,1)S(1)}, bf16[192,512]{1,0:T(8,128)(2,1)}, u32[]{:S(2)}) copy-start(bf16[192,512]{1,0:T(8,128)(2,1)} %cot_ref.1) | copy-start | bytes 589828
  0.7 6.0 %copy-start.6 = (f32[192,2]{0,1:T(2,128)S(1)}, f32[192,2]{0,1:T(2,128)}, u32[]{:S(2)}) copy-start(f32[192,2]{0,1:T(2,128)} %param.17) | copy-start | bytes 4612
  3.7 4.6 %copy-start.14 = (bf16[192,512]{1,0:T(8,128)(2,1)S(1)}, bf16[192,512]{1,0:T(8,128)(2,1)}, u32[]{:S(2)}) copy-start(bf16[192,512]{1,0:T(8,128)(2,1)} %param.14) | copy-start | bytes 589828
  51.9 5.5 %copy-start.9 = (bf16[1,2048,896]{2,1,0:T(8,128)(2,1)S(1)}, bf16[1,2048,896]{2,1,0:T(8,128)(2,1)}, u32[]{:S(2)}) copy-start(bf16[1,2048,896]{2,1,0:T(8,128)(2,1)} %param.19) | copy-start | bytes 11010052
  51.9 5.5 %copy-start.10 = (bf16[8,72,2048]{2,1,0:T(8,128)(2,1)S(1)}, bf16[8,72,2048]{2,1,0:T(8,128)(2,1)}, u32[]{:S(2)}) copy-start(bf16[8,72,2048]{2,1,0:T(8,128)(2,1)} %get-tuple-element.12) | copy-start | bytes 7077892
  57.4 2.6 %copy-start.17 = (f32[576,896]{1,0:T(8,128)}, f32[576,896]{1,0:T(8,128)S(1)}, u32[]{:S(2)}) copy-start(f32[576,896]{1,0:T(8,128)S(1)} %fusion.2) | copy-start | bytes 6193156
  57.4 2.8 %copy-start.7 = (bf16[1,896,2048]{2,1,0:T(8,128)(2,1)S(1)}, bf16[1,896,2048]{2,1,0:T(8,128)(2,1)}, u32[]{:S(2)}) copy-start(bf16[1,896,2048]{2,1,0:T(8,128)(2,1)} %param.20) | copy-start | bytes 11010052
  57.4 3.5 %copy-start.12 = (bf16[8,72,2048]{2,1,0:T(8,128)(2,1)S(1)}, bf16[8,72,2048]{2,1,0:T(8,128)(2,1)}, u32[]{:S(2)}) copy-start(bf16[8,72,2048]{2,1,0:T(8,128)(2,1)} %get-tuple-element.13) | copy-start | bytes 7077892
  60.0 4.1 %copy-start.18 = (f32[576,896]{1,0:T(8,128)}, f32[576,896]{1,0:T(8,128)S(1)}, u32[]{:S(2)}) copy-start(f32[576,896]{1,0:T(8,128)S(1)} %fusion.6) | copy-start | bytes 6193156
  60.9 3.3 %copy-start.8 = (bf16[1,2048,896]{2,1,0:T(8,128)(2,1)S(1)}, bf16[1,2048,896]{2,1,0:T(8,128)(2,1)}, u32[]{:S(2)}) copy-start(bf16[1,2048,896]{2,1,0:T(8,128)(2,1)} %param.18) | copy-start | bytes 11010052
  64.2 2.7 %copy-start.19 = (bf16[576,896]{1,0:T(8,128)(2,1)}, bf16[576,896]{1,0:T(8,128)(2,1)S(1)}, u32[]{:S(2)}) copy-start(bf16[576,896]{1,0:T(8,128)(2,1)S(1)} %get-tuple-element.22) | copy-start | bytes 3096580
  70.8 41.0 %copy-start.15 = (f32[192,256]{1,0:T(8,128)S(1)}, f32[192,256]{1,0:T(8,128)}, u32[]{:S(2)}) copy-start(f32[192,256]{1,0:T(8,128)} %get-tuple-element.14) | copy-start | bytes 589828
  70.8 41.0 %copy-start.16 = (bf16[192,256]{1,0:T(8,128)(2,1)S(1)}, bf16[192,256]{1,0:T(8,128)(2,1)}, u32[]{:S(2)}) copy-start(bf16[192,256]{1,0:T(8,128)(2,1)} %param.23) | copy-start | bytes 294916
  114.5 32.0 %copy-start.2 = (bf16[192,256]{1,0:T(8,128)(2,1)S(1)}, bf16[192,256]{1,0:T(8,128)(2,1)}, u32[]{:S(2)}) copy-start(bf16[192,256]{1,0:T(8,128)(2,1)} %param.22) | copy-start | bytes 294916
  114.5 32.0 %copy-start.4 = (f32[192,256]{1,0:T(8,128)S(1)}, f32[192,256]{1,0:T(8,128)}, u32[]{:S(2)}) copy-start(f32[192,256]{1,0:T(8,128)} %get-tuple-element.17) | copy-start | bytes 589828
  146.4 5.2 %copy-start.13 = (bf16[8,72,2048]{2,1,0:T(8,128)(2,1)S(1)}, bf16[8,72,2048]{2,1,0:T(8,128)(2,1)}, u32[]{:S(2)}) copy-start(bf16[8,72,2048]{2,1,0:T(8,128)(2,1)} %get-tuple-element.13) | copy-start | bytes 7077892
  151.6 7.0 %copy-start.11 = (bf16[8,72,2048]{2,1,0:T(8,128)(2,1)S(1)}, bf16[8,72,2048]{2,1,0:T(8,128)(2,1)}, u32[]{:S(2)}) copy-start(bf16[8,72,2048]{2,1,0:T(8,128)(2,1)} %get-tuple-element.12) | copy-start | bytes 7077892
  151.6 7.0 %copy-start.20 = (bf16[576,896]{1,0:T(8,128)(2,1)S(1)}, bf16[576,896]{1,0:T(8,128)(2,1)}, u32[]{:S(2)}) copy-start(bf16[576,896]{1,0:T(8,128)(2,1)} %copy-done.19) | copy-start | bytes 3096580
  163.5 4.8 %copy-start.3 = (f32[256,256]{1,0:T(8,128)S(1)}, f32[256,256]{1,0:T(8,128)}, u32[]{:S(2)}) copy-start(f32[256,256]{1,0:T(8,128)} %get-tuple-element.41) | copy-start | bytes 786436

commit v2 on v1

--- a/solution.py
+++ b/solution.py
@@ -13,6 +13,25 @@
 def partner(t, stage, m):
     d = m >> (stage + 1)
     return t + d * (1 - 2 * ((t // d) % 2))
+
+
+def flipped(s, j, n):
+    out = 0
+    for b in range(n.bit_length() - 1):
+        bit = (s // 2**b) % 2
+        out = out + (1 - bit if (j >> b) % 2 else bit) * 2**b
+    return out
+
+
+def far_near(n):
+    near, far = list(range(n // 2)), list(range(n // 2, n))
+    arrive = near[:1]
+    for i in range(1, n // 2):
+        arrive += [near[i], far[i - 1]]
+    leave = []
+    for i in range(1, n // 2):
+        leave += [far[i - 1], near[i]]
+    return arrive + far[-1:], leave + far[-1:], far + near[1:] + near[:1]
 
 
 def held_columns(t, stage, m):
@@ -89,9 +108,10 @@
     def block(a, src, col):
         return targets[a].at[src, :, pl.ds(pl.multiple_of(col * feat, feat), feat)]
 
-    first = []
-    for k in range(n):
-        dst = lax.rem(s + k, n)
+    first = {}
+    arrive, leave, _ = far_near(n)
+    for k in [0] + leave:
+        dst = flipped(s, k, n)
         for a in range(2):
             if k == 0:
                 copy = pltpu.make_async_copy(sources[a].at[s], block(a, s, t), self_sem.at[a])
@@ -104,12 +124,12 @@
                     {"sp": dst},
                 )
             copy.start()
-            first.append(copy)
+            first[k, a] = copy
 
     pushed = []
 
     def push(a, k, stage, i, col):
-        src = lax.rem(s + n - k, n)
+        src = flipped(s, k, n)
         at = 2**stage - 1 + i
         copy = remote(
             block(a, src, col),
@@ -122,7 +142,7 @@
         pushed.append(copy)
 
     def arrived(k, stage):
-        src = lax.rem(s + n - k, n)
+        src = flipped(s, k, n)
         cols = held_columns(partner(t, stage, m), stage, m)
         for i, col in enumerate(cols):
             at = 2**stage - 1 + i
@@ -140,20 +160,20 @@
     def forward(k):
         for a in range(2):
             if k == 0:
-                first[a].wait()
+                first[k, a].wait()
             else:
-                first[2 * k + a].wait_recv()
+                first[k, a].wait_recv()
             for stage in range(stages):
                 push(a, k, stage, 0, t)
 
-    forward(0)
+    forward(arrive[0])
     gain, term = local_scan(decay_ref[...], driven_ref[...], False)
     gain_buf[...] = gain
     states_ref[...] = term
     rows = gain.shape[0]
     car_send[0:1] = gain[rows - 1 : rows]
     car_send[1:2] = term[rows - 1 : rows]
-    forward(1)
+    forward(arrive[1])
     carries = []
     for k in range(1, n):
         copy = remote(
@@ -161,10 +181,10 @@
         )
         copy.start()
         carries.append(copy)
-    for k in range(2, n):
-        forward(k)
+    for at in range(2, n):
+        forward(arrive[at])
         for stage in range(stages - 1):
-            arrived(k - 2, stage)
+            arrived(arrive[at - 2], stage)
     for copy in carries:
         copy.wait()
     carry = jnp.zeros((1, gain_buf.shape[1]), jnp.float32)
@@ -173,13 +193,14 @@
     states = states_ref[...] + gain_buf[...] * carry
     states_ref[...] = states
     prev_ref[...] = jnp.concatenate([carry, states[:-1]], axis=0)
-    for k in range(n - 2, n):
+    for k in arrive[n - 2 :]:
         for stage in range(stages - 1):
             arrived(k, stage)
     for k in range(n):
         arrived(k, stages - 1)
-    for copy in first[2:]:
-        copy.wait_send()
+    for k in leave:
+        for a in range(2):
+            first[k, a].wait_send()
     for copy in pushed:
         copy.wait_send()
 
@@ -251,11 +272,11 @@
         base.append(total)
         total += m >> (stage + 1)
 
-    order = list(range(1, n)) + [0]
+    order = far_near(n)[2]
     waits = []
 
     def send_stage(k, stage):
-        dst = lax.rem(s + k, n)
+        dst = flipped(s, k, n)
         source = part_ref if stage == 0 else acc_buf
         peer = across(stage)
         step = 2 ** (stage + 1)
@@ -273,7 +294,7 @@
             waits.append(copy)
 
     def sum_stage(k, stage):
-        dst = lax.rem(s + k, n)
+        dst = flipped(s, k, n)
         source = part_ref if stage == 0 else acc_buf
         step = 2 ** (stage + 1)
         for i in range(m // step):
@@ -292,7 +313,7 @@
             )
 
     def send_home(k):
-        dst = lax.rem(s + k, n)
+        dst = flipped(s, k, n)
         if k == 0:
             back_buf[s] = acc_buf[s, :, cols(t)]
             return
@@ -318,8 +339,8 @@
                 else:
                     send_home(k)
     value = cot_ref[...].astype(jnp.float32)
-    for k in range(n):
-        src = lax.rem(s + n - k, n)
+    for k in [0] + order[:-1]:
+        src = flipped(s, k, n)
         if k > 0:
             remote(
                 acc_buf.at[src, :, cols(t)],
@@ -396,6 +417,7 @@
     car_send,
     car_buf,
     part_buf,
+    pair_buf,
     part_ssem,
     part_rsem,
     car_ssem,
@@ -403,13 +425,16 @@
 ):
     s = lax.axis_index("sp")
     greet([{"sp": lax.rem(s + k, n)} for k in range(1, n)])
-    parts = []
-    for k in range(1, n):
-        dst = lax.rem(s + k, n)
-        copy = remote(
-            part_ref.at[dst], part_buf.at[k], part_ssem.at[k], part_rsem.at[k], {"sp": dst}
-        )
-        parts.append(copy)
+    beside = flipped(s, 1, n)
+    half = n // 2
+    order = [half - 1 - j for j in range(half)]
+    near = {}
+    for j in order:
+        dst = flipped(s, 2 * j + 1, n)
+        near[j] = remote(
+            part_ref.at[dst], part_buf.at[j], part_ssem.at[j], part_rsem.at[j], {"sp": beside}
+        )
+        near[j].start()
     decay = decay_ref[...]
     gain, term = local_scan(shifted(decay, 1, 1.0, True), input_ref[...], True)
     gain_buf[...] = gain
@@ -423,18 +448,33 @@
         )
         copy.start()
         carries.append(copy)
-    for copy in parts:
-        copy.start()
+    far = {}
+    for j in order:
+        near[j].wait_recv()
+        home = flipped(s, 2 * j, n)
+        both = part_ref[home].astype(jnp.float32) + part_buf[j].astype(jnp.float32)
+        if j == 0:
+            sum_ref[...] = both
+            continue
+        pair_buf[j] = both.astype(jnp.bfloat16)
+        at = half + j
+        far[j] = remote(
+            pair_buf.at[j], part_buf.at[at], part_ssem.at[at], part_rsem.at[at], {"sp": home}
+        )
+        far[j].start()
     for copy in carries:
         copy.wait()
     carry = jnp.zeros((1, gain_buf.shape[1]), jnp.float32)
     for k in range(1, n):
         carry = jnp.where(k > s, car_buf[k, 0:1] * carry + car_buf[k, 1:2], carry)
     grad_ref[...] = grad_ref[...] + gain_buf[...] * carry
-    sum_ref[...] = part_ref[s].astype(jnp.float32)
-    for k in range(1, n):
-        parts[k - 1].wait()
-        sum_ref[...] += part_buf[k].astype(jnp.float32)
+    for j in order[:-1]:
+        far[j].wait_recv()
+        sum_ref[...] += part_buf[half + j].astype(jnp.float32)
+    for j in order:
+        near[j].wait_send()
+    for j in order[:-1]:
+        far[j].wait_send()
 
 
 def tail(decay, state_in, part):
@@ -454,6 +494,7 @@
             pltpu.VMEM((2, channels), jnp.float32),
             pltpu.VMEM((n, 2, channels), jnp.float32),
             pltpu.VMEM(part.shape, part.dtype),
+            pltpu.VMEM((n // 2,) + part.shape[1:], part.dtype),
             pltpu.SemaphoreType.DMA((n,)),
             pltpu.SemaphoreType.DMA((n,)),
             pltpu.SemaphoreType.DMA((n,)),

time: 170 us -> 155 us (0.912)
  the two profiles are of different devices: /device:TPU:12 before, /device:TPU:0 now
where the time goes in v2:
time: 155 us
  Pallas kernels  98.1 us (63%)
  matrix products  46.5 us (30%)
  other arithmetic  7.01 us (5%)
  local copies, waits for them, and re-layouts  2.47 us (2%)
    pallas_call x1, Pallas kernels, dispatch(): pl.pallas_call(functools.partial(dispatch_kernel, n, m), out_shape=(whole...  43.1 us
    pallas_call x1, Pallas kernels, bring_back(): pl.pallas_call(functools.partial(return_kernel, n, m), out_shape=jax.Shap...  32.4 us
    pallas_call x1, Pallas kernels, tail(): pl.pallas_call(functools.partial(tail_kernel, n), out_shape=(jax.ShapeDty...  22.6 us
    dot_general x1, matrix products, expert_backward(): lax.dot_general(hidden, cotangent, (((0,), (0,)), ((), ())), preferred_el...  7.02 us
    dot_general x1, matrix products, expert_backward(): gate_act = jnp.dot(inputs, gate_weight, preferred_element_type=jnp.float32)  5.49 us
    dot_general x1, matrix products, expert_backward(): lax.dot_general(inputs, d_up, (((0,), (0,)), ((), ())), preferred_element...  4.84 us
    dot_general x1, matrix products, expert_backward(): lax.dot_general(inputs, d_gate, (((0,), (0,)), ((), ())), preferred_eleme...  4.84 us
    dot_general x1, matrix products, expert_backward(): lax.dot_general(d_up, up_weight, (((1,), (1,)), ((), ())), preferred_elem...  3.89 us

profile of v2, /device:TPU:0, one launch (start us, length us, event | category | flops | bytes accessed | tf_op | source)
XLA Modules:
  0.0 155.0 jit_solution(5859017065044662931)
XLA Ops:
  0.7 1.2 fusion.17
  1.9 1.1 fusion.21
  3.0 0.7 fusion.90
  3.7 1.8 %fusion.63 = (f32[192,256]{1,0:T(8,128)}, f32[192,256]{1,0:T(8,128)S(1)}) fusion(f32[2,24,8,128]{3,2,1,0:T(8,128)S(1)} %fusion.17, bf16[192,256]{1,0:T(8,128)(2,1)} %param.22, f32[192,256]{1,0:T(8,128)} %param.27, f32[256]{0:T(256)S(1)} %fusion.90, f32[2,24,8,128]{3,2,1,0:T(8,128)S(1)} %fusion.21), kind=kLoop, calls=%fused_computation.94 | loop fusion | flops 344064 | bytes 1082368 | tf_op jit(solution)/shard_map/mul | solution.py:614
  5.5 0.7 exp.22.decay_ref
  6.2 0.2 select_reduce_fusion.1
  6.4 0.2 broadcast_compare_fusion.1
  6.7 0.1 mul.170
  6.8 0.1 fusion.27
  6.9 1.3 fusion.23.cot_ref
  8.3 1.1 fusion.34
  9.4 43.1 %dispatch.1 = (bf16[8,72,2048]{2,1,0:T(8,128)(2,1)}, bf16[8,72,2048]{2,1,0:T(8,128)(2,1)}, f32[192,256]{1,0:T(8,128)}, f32[192,256]{1,0:T(8,128)}) custom-call(bf16[8,72,512]{2,1,0:T(8,128)(2,1)} %bitcast.120, bf16[8,72,512]{2,1,0:T(8,128)(2,1)} %fusion.23.cot_ref, f32[192,256]{1,0:T(8,128)} %exp.22.decay_ref, f32[192,256]{1,0:T(8,128)} %get-tuple-element.20.driven_ref), custom_call_target="tpu_custom_call" | custom-call | tf_op jit(solution)/shard_map/dispatch/pallas_call | solution.py:215
  52.6 5.5 %fusion.2 = f32[576,896]{1,0:T(8,128)S(1)} fusion(bf16[576,2048]{1,0:T(8,128)(2,1)} %bitcast.125, bf16[1,2048,896]{2,1,0:T(8,128)(2,1)} %param.18), kind=kOutput, calls=%fused_computation.3 | convolution fusion | flops 2113929216 | bytes 8093696 | tf_op jit(solution)/shard_map/dot_general | solution.py:514
  58.1 2.6 %fusion.6 = f32[576,896]{1,0:T(8,128)S(1)} fusion(bf16[576,2048]{1,0:T(8,128)(2,1)S(1)} %bitcast.126, bf16[1,2048,896]{2,1,0:T(8,128)(2,1)S(1)} %copy-done.9), kind=kOutput, calls=%fused_computation.7 | convolution fusion | flops 2113929216 | bytes 8093696 | tf_op jit(solution)/shard_map/dot_general | solution.py:515
  60.7 0.1 copy-done.7
  60.9 0.7 copy-done.12
  61.6 3.2 %multiply_convert_fusion.1 = (bf16[576,896]{1,0:T(8,128)(2,1)S(1)}, bf16[576,896]{1,0:T(8,128)(2,1)S(1)}) fusion(f32[576,896]{1,0:T(8,128)S(1)} %fusion.2, f32[576,896]{1,0:T(8,128)S(1)} %fusion.6, bf16[576,2048]{1,0:T(8,128)(2,1)S(1)} %bitcast.129, bf16[1,896,2048]{2,1,0:T(8,128)(2,1)S(1)} %copy-done.7), kind=kOutput, calls=%fused_computation.16 | convolution fusion | flops 2120638464 | bytes 12222464 | tf_op jit(solution)/shard_map/dot_general | solution.py:519
  64.9 2.6 %fusion = f32[576,2048]{1,0:T(8,128)S(1)} fusion(bf16[576,896]{1,0:T(8,128)(2,1)S(1)} %get-tuple-element.23, bf16[1,2048,896]{2,1,0:T(8,128)(2,1)S(1)} %copy-done.8), kind=kOutput, calls=%fused_computation.1 | convolution fusion | flops 2113929216 | bytes 9420800 | tf_op jit(solution)/shard_map/dot_general | solution.py:535
  67.5 3.9 %add_convert_fusion = bf16[576,2048]{1,0:T(8,128)(2,1)} fusion(f32[576,2048]{1,0:T(8,128)S(1)} %fusion, bf16[576,896]{1,0:T(8,128)(2,1)S(1)} %get-tuple-element.22, bf16[1,2048,896]{2,1,0:T(8,128)(2,1)S(1)} %copy-done.9), kind=kOutput, calls=%fused_computation | convolution fusion | flops 2116288512 | bytes 11780096 | tf_op jit(solution)/shard_map/dot_general | solution.py:538
  71.4 1.0 fusion.30.pick_ref
  72.4 32.4 %bring_back.1 = bf16[192,2048]{1,0:T(8,128)(2,1)} custom-call(bf16[8,72,2048]{2,1,0:T(8,128)(2,1)} %bitcast.118, bf16[8,192,72]{2,1,0:T(8,128)(2,1)} %fusion.30.pick_ref, bf16[192,512]{1,0:T(8,128)(2,1)} %cot_ref.1), custom_call_target="tpu_custom_call" | custom-call | tf_op jit(solution)/shard_map/bring_back/pallas_call | solution.py:388
  104.8 2.6 %convolution_convert_fusion = bf16[2048,256]{1,0:T(8,128)(2,1)} fusion(bf16[192,2048]{1,0:T(8,128)(2,1)} %bring_back.1, f32[192,256]{1,0:T(8,128)S(1)} %copy-done.15, bf16[192,256]{1,0:T(8,128)(2,1)S(1)} %copy-done.16), kind=kOutput, calls=%fused_computation.14 | convolution fusion | flops 202391552 | bytes 2129920 | tf_op jit(solution)/shard_map/dot_general | solution.py:635
  107.4 2.3 %fusion.58 = (f32[192,256]{1,0:T(8,128)}, f32[192,256]{1,0:T(8,128)}) fusion(bf16[192,256]{1,0:T(8,128)(2,1)S(1)} %copy-done.16, f32[192,256]{1,0:T(8,128)S(1)} %copy-done.15, bf16[192,2048]{1,0:T(8,128)(2,1)} %bring_back.1, bf16[2048,256]{1,0:T(8,128)(2,1)S(1)} %copy-done), kind=kOutput, calls=%fused_computation.81 | convolution fusion | flops 202358784 | bytes 2523136 | tf_op jit(solution)/shard_map/dot_general | solution.py:632
  109.8 22.6 %tail.1 = (f32[192,256]{1,0:T(8,128)}, f32[256,256]{1,0:T(8,128)}) custom-call(f32[192,256]{1,0:T(8,128)} %exp.22.decay_ref, f32[192,256]{1,0:T(8,128)} %get-tuple-element.27.input_ref, bf16[8,256,256]{2,1,0:T(8,128)(2,1)} %bitcast.119), custom_call_target="tpu_custom_call" | custom-call | tf_op jit(solution)/shard_map/tail/pallas_call | solution.py:484
  132.4 1.3 fusion.64
  133.7 1.0 fusion.67
  134.8 1.0 fusion.13
  135.8 1.7 %bitcast_add_fusion = f32[192,256]{1,0:T(8,128)} fusion(f32[2,24,8,128]{3,2,1,0:T(8,128)S(1)} %fusion.13, f32[192,256]{1,0:T(8,128)} %get-tuple-element.16, f32[2,24,8,128]{3,2,1,0:T(8,128)S(1)} %fusion.17, f32[192,256]{1,0:T(8,128)S(1)} %get-tuple-element.21), kind=kLoop, calls=%fused_computation.82 | loop fusion | flops 245760 | bytes 983040 | tf_op jit(solution)/shard_map/add | solution.py:663
  137.5 7.0 %convert_bitcast_fusion = bf16[1,896,2048]{2,1,0:T(8,128)(2,1)} fusion(bf16[576,2048]{1,0:T(8,128)(2,1)S(1)} %bitcast.130, f32[576,896]{1,0:T(8,128)} %copy-done.18, f32[576,896]{1,0:T(8,128)} %copy-done.17), kind=kOutput, calls=%fused_computation.11 | convolution fusion | flops 2118860800 | bytes 10158080 | tf_op jit(solution)/shard_map/dot_general | solution.py:522
  144.6 4.8 %convert_bitcast_fusion.1 = bf16[1,2048,896]{2,1,0:T(8,128)(2,1)} fusion(bf16[576,2048]{1,0:T(8,128)(2,1)S(1)} %bitcast.127, bf16[576,896]{1,0:T(8,128)(2,1)S(1)} %copy-done.20), kind=kOutput, calls=%fused_computation.12 | convolution fusion | flops 2115764224 | bytes 7061504 | tf_op jit(solution)/shard_map/dot_general | solution.py:532
  149.4 4.8 %convert_bitcast_fusion.2 = bf16[1,2048,896]{2,1,0:T(8,128)(2,1)} fusion(bf16[576,2048]{1,0:T(8,128)(2,1)S(1)} %bitcast.128, bf16[576,896]{1,0:T(8,128)(2,1)S(1)} %get-tuple-element.23), kind=kOutput, calls=%fused_computation.13 | convolution fusion | flops 2115764224 | bytes 7061504 | tf_op jit(solution)/shard_map/dot_general | solution.py:529
  154.2 0.7 copy.67
  (44 shorter events, 0.1 us)
Async XLA Ops:
  0.6 106.8 %copy-start = (bf16[2048,256]{1,0:T(8,128)(2,1)S(1)}, bf16[2048,256]{1,0:T(8,128)(2,1)}, u32[]{:S(2)}) copy-start(bf16[2048,256]{1,0:T(8,128)(2,1)} %param.21) | copy-start | bytes 3145732
  0.6 5.6 %copy-start.5 = (s32[192,2]{0,1:T(2,128)S(1)}, s32[192,2]{0,1:T(2,128)}, u32[]{:S(2)}) copy-start(s32[192,2]{0,1:T(2,128)} %param.16) | copy-start | bytes 4612
  0.7 6.0 %copy-start.1 = (bf16[192,512]{1,0:T(8,128)(2,1)S(1)}, bf16[192,512]{1,0:T(8,128)(2,1)}, u32[]{:S(2)}) copy-start(bf16[192,512]{1,0:T(8,128)(2,1)} %cot_ref.1) | copy-start | bytes 589828
  0.7 6.0 %copy-start.6 = (f32[192,2]{0,1:T(2,128)S(1)}, f32[192,2]{0,1:T(2,128)}, u32[]{:S(2)}) copy-start(f32[192,2]{0,1:T(2,128)} %param.17) | copy-start | bytes 4612
  3.7 4.6 %copy-start.14 = (bf16[192,512]{1,0:T(8,128)(2,1)S(1)}, bf16[192,512]{1,0:T(8,128)(2,1)}, u32[]{:S(2)}) copy-start(bf16[192,512]{1,0:T(8,128)(2,1)} %param.14) | copy-start | bytes 589828
  52.5 5.5 %copy-start.9 = (bf16[1,2048,896]{2,1,0:T(8,128)(2,1)S(1)}, bf16[1,2048,896]{2,1,0:T(8,128)(2,1)}, u32[]{:S(2)}) copy-start(bf16[1,2048,896]{2,1,0:T(8,128)(2,1)} %param.19) | copy-start | bytes 11010052
  52.6 5.5 %copy-start.10 = (bf16[8,72,2048]{2,1,0:T(8,128)(2,1)S(1)}, bf16[8,72,2048]{2,1,0:T(8,128)(2,1)}, u32[]{:S(2)}) copy-start(bf16[8,72,2048]{2,1,0:T(8,128)(2,1)} %get-tuple-element.12) | copy-start | bytes 7077892
  58.1 2.6 %copy-start.17 = (f32[576,896]{1,0:T(8,128)}, f32[576,896]{1,0:T(8,128)S(1)}, u32[]{:S(2)}) copy-start(f32[576,896]{1,0:T(8,128)S(1)} %fusion.2) | copy-start | bytes 6193156
  58.1 2.8 %copy-start.7 = (bf16[1,896,2048]{2,1,0:T(8,128)(2,1)S(1)}, bf16[1,896,2048]{2,1,0:T(8,128)(2,1)}, u32[]{:S(2)}) copy-start(bf16[1,896,2048]{2,1,0:T(8,128)(2,1)} %param.20) | copy-start | bytes 11010052
  58.1 3.5 %copy-start.12 = (bf16[8,72,2048]{2,1,0:T(8,128)(2,1)S(1)}, bf16[8,72,2048]{2,1,0:T(8,128)(2,1)}, u32[]{:S(2)}) copy-start(bf16[8,72,2048]{2,1,0:T(8,128)(2,1)} %get-tuple-element.13) | copy-start | bytes 7077892
  60.7 4.1 %copy-start.18 = (f32[576,896]{1,0:T(8,128)}, f32[576,896]{1,0:T(8,128)S(1)}, u32[]{:S(2)}) copy-start(f32[576,896]{1,0:T(8,128)S(1)} %fusion.6) | copy-start | bytes 6193156
  61.6 3.3 %copy-start.8 = (bf16[1,2048,896]{2,1,0:T(8,128)(2,1)S(1)}, bf16[1,2048,896]{2,1,0:T(8,128)(2,1)}, u32[]{:S(2)}) copy-start(bf16[1,2048,896]{2,1,0:T(8,128)(2,1)} %param.18) | copy-start | bytes 11010052
  64.9 2.7 %copy-start.19 = (bf16[576,896]{1,0:T(8,128)(2,1)}, bf16[576,896]{1,0:T(8,128)(2,1)S(1)}, u32[]{:S(2)}) copy-start(bf16[576,896]{1,0:T(8,128)(2,1)S(1)} %get-tuple-element.22) | copy-start | bytes 3096580
  71.4 33.4 %copy-start.15 = (f32[192,256]{1,0:T(8,128)S(1)}, f32[192,256]{1,0:T(8,128)}, u32[]{:S(2)}) copy-start(f32[192,256]{1,0:T(8,128)} %get-tuple-element.14) | copy-start | bytes 589828
  71.4 33.4 %copy-start.16 = (bf16[192,256]{1,0:T(8,128)(2,1)S(1)}, bf16[192,256]{1,0:T(8,128)(2,1)}, u32[]{:S(2)}) copy-start(bf16[192,256]{1,0:T(8,128)(2,1)} %param.23) | copy-start | bytes 294916
  107.4 24.9 %copy-start.2 = (bf16[192,256]{1,0:T(8,128)(2,1)S(1)}, bf16[192,256]{1,0:T(8,128)(2,1)}, u32[]{:S(2)}) copy-start(bf16[192,256]{1,0:T(8,128)(2,1)} %param.22) | copy-start | bytes 294916
  107.4 24.9 %copy-start.4 = (f32[192,256]{1,0:T(8,128)S(1)}, f32[192,256]{1,0:T(8,128)}, u32[]{:S(2)}) copy-start(f32[192,256]{1,0:T(8,128)} %get-tuple-element.17) | copy-start | bytes 589828
  132.4 5.2 %copy-start.13 = (bf16[8,72,2048]{2,1,0:T(8,128)(2,1)S(1)}, bf16[8,72,2048]{2,1,0:T(8,128)(2,1)}, u32[]{:S(2)}) copy-start(bf16[8,72,2048]{2,1,0:T(8,128)(2,1)} %get-tuple-element.13) | copy-start | bytes 7077892
  137.5 7.0 %copy-start.11 = (bf16[8,72,2048]{2,1,0:T(8,128)(2,1)S(1)}, bf16[8,72,2048]{2,1,0:T(8,128)(2,1)}, u32[]{:S(2)}) copy-start(bf16[8,72,2048]{2,1,0:T(8,128)(2,1)} %get-tuple-element.12) | copy-start | bytes 7077892
  137.5 7.0 %copy-start.20 = (bf16[576,896]{1,0:T(8,128)(2,1)S(1)}, bf16[576,896]{1,0:T(8,128)(2,1)}, u32[]{:S(2)}) copy-start(bf16[576,896]{1,0:T(8,128)(2,1)} %copy-done.19) | copy-start | bytes 3096580
  149.4 4.8 %copy-start.3 = (f32[256,256]{1,0:T(8,128)S(1)}, f32[256,256]{1,0:T(8,128)}, u32[]{:S(2)}) copy-start(f32[256,256]{1,0:T(8,128)} %get-tuple-element.41) | copy-start | bytes 786436
